TPU v7x, 768 devices: a whole 4x8x12 slice. The times are simulated.
768 devices in a mesh: ep: 48 (over z, x), tp: 16 (over y, core).
Axes of the slice: x: 4, y: 8, z: 12, core: 2. Of those that a mesh axis runs over, the one named last changes fastest.
Arguments:
- tokens: bfloat16 [9216, 2048], P('ep'), may hold values from -6 to 6
- cotangent: bfloat16 [9216, 2048], P('ep'), may hold values from -6 to 6
- routing: int32 [9216, 2], P('ep'), may hold values from 0 to 47, all different within a row; in each aligned block of 192 rows (0 to 191, 192 to 383, ...) at most 10 rows name the same one
- route_weights: float32 [9216, 2], P('ep'), may hold values from 0.1 to 1
- w_gate: bfloat16 [48, 2048, 2048], P('ep', None, 'tp'), may hold values from -0.125 to 0.125
- w_up: bfloat16 [48, 2048, 2048], P('ep', None, 'tp'), may hold values from -0.125 to 0.125
- w_down: bfloat16 [48, 2048, 2048], P('ep', 'tp'), may hold values from -0.125 to 0.125
Outputs:
- grad_tokens: bfloat16 [9216, 2048], P('ep')
- grad_weights: bfloat16 [9216, 2], P('ep')
- grad_gate: bfloat16 [48, 2048, 2048], P('ep', None, 'tp')
- grad_up: bfloat16 [48, 2048, 2048], P('ep', None, 'tp')
- grad_down: bfloat16 [48, 2048, 2048], P('ep', 'tp')
Inputs may be any that keep to these rules, and one draw needn't show every extreme that they name: `routing`: each row names 2 different experts. Within the rows of one device no expert is named more than 10 times, and in every draw some expert is named exactly 10 times by some device's rows.
All inputs are finite; a program needn't handle non-finite values.
Results may differ from a plain program's by a relative error of at most 0.019.
Values may be sent and summed in bfloat16 or wider, within the bound.
A program may use at most 64 MiB of HBM per device.

v0:
```python
import jax
import jax.numpy as jnp
from jax import lax
from jax.sharding import PartitionSpec as P


def in_one_piece(arrays, axis, split_dim, concat_dim, along):
    columns = [a.reshape(*a.shape[:along], -1) for a in arrays]
    both = jnp.concatenate(columns, axis=along)
    filled, at, done = (
        lax.all_to_all(both, axis, split_axis=split_dim, concat_axis=concat_dim, tiled=True),
        0,
        [],
    )
    for a, column in zip(arrays, columns):
        slab = filled[..., at : at + column.shape[along]]
        done.append(slab.reshape(*slab.shape[:along], *a.shape[along:]))
        at += column.shape[along]
    return tuple(done)


def in_one_piece_2(arrays, axis, dim, along):
    ends, at = ([], 0)
    for a in arrays[:-1]:
        at += a.shape[along]
        ends.append(at)
    both = jnp.concatenate(arrays, axis=along)
    return tuple(jnp.split(lax.all_gather(both, axis, axis=dim, tiled=True), ends, axis=along))


def split_up(x, dim, size):
    before, after = (x.shape[:dim], x.shape[dim + 1 :])
    return jnp.moveaxis(x.reshape(*before, size, -1, *after), dim, 0)


def sum_at_owner(x, axis, dim):
    tiles = split_up(x, dim, lax.axis_size(axis))
    arrived = lax.all_to_all(tiles, axis, split_axis=0, concat_axis=0, tiled=True)
    return arrived.astype(jnp.float32).sum(axis=0)


def from_everyone(x, axis):
    copies = jnp.broadcast_to(x, (lax.axis_size(axis), *x.shape))
    return lax.all_to_all(copies, axis, split_axis=0, concat_axis=0, tiled=True)


def taken_together(x, axis):
    everything = from_everyone(x, axis)
    return jnp.sum(everything.astype(jnp.float32), axis=0)


def in_order(tiles, dim):
    shape = list(tiles.shape[1:])
    shape[dim] *= tiles.shape[0]
    return jnp.moveaxis(tiles, 0, dim).reshape(shape)


def gathered_copies(x, axis, dim):
    tiles = from_everyone(x, axis)
    return in_order(tiles, dim)


def slot_tables(routing, experts, capacity):
    flat = routing.reshape(-1)
    onehot = (flat[:, None] == jnp.arange(experts, dtype=jnp.int32)[None, :]).astype(jnp.int32)
    before = jnp.cumsum(onehot, axis=0) - onehot
    within = jnp.sum(before * onehot, axis=1)
    target = flat * capacity + within
    chosen = jnp.arange(experts * capacity, dtype=jnp.int32)[:, None] == target[None, :]
    return (target, chosen)


def on_device(tokens, cotangent, routing, route_weights, w_gate, w_up, w_down):
    experts = lax.axis_size("ep")
    local_tokens, top_count = routing.shape
    width = tokens.shape[1]
    capacity = max(2, (5 * local_tokens * top_count + 4 * experts - 1) // (4 * experts))
    slot_total = experts * capacity
    target, chosen = slot_tables(routing, experts, capacity)
    picked = chosen.reshape(slot_total, local_tokens, top_count).astype(jnp.float32)
    by_token = jnp.sum(picked, axis=2).astype(jnp.bfloat16)
    slot_weight = jnp.sum(picked * route_weights[None, :, :], axis=(1, 2)).astype(jnp.bfloat16)
    piece = width // lax.axis_size("tp")
    start = lax.axis_index("tp") * piece
    token_cols = lax.dynamic_slice_in_dim(tokens, start, piece, 1)
    back_cols = lax.dynamic_slice_in_dim(cotangent, start, piece, 1)
    send_rows = jnp.dot(by_token, token_cols, preferred_element_type=jnp.float32).astype(
        jnp.bfloat16
    )
    send_back = jnp.dot(by_token, back_cols, preferred_element_type=jnp.float32).astype(
        jnp.bfloat16
    )
    rows_cols, back_part, weight_in = in_one_piece(
        (
            send_rows.reshape(experts, capacity, piece),
            send_back.reshape(experts, capacity, piece),
            slot_weight.reshape(experts, capacity),
        ),
        "ep",
        0,
        0,
        2,
    )
    rows_in, back_in = in_one_piece_2((rows_cols, back_part), "tp", 2, 0)
    rows = rows_in.reshape(slot_total, width)
    back = back_in.reshape(slot_total, width)
    weight = weight_in.reshape(slot_total, 1).astype(jnp.float32)
    wgate = w_gate[0]
    wup = w_up[0]
    wdown = w_down[0]
    pre_gate = jnp.dot(rows, wgate, preferred_element_type=jnp.float32)
    pre_up = jnp.dot(rows, wup, preferred_element_type=jnp.float32)
    along = jnp.einsum("rd,fd->rf", back, wdown, preferred_element_type=jnp.float32)
    gate_sig = jax.nn.sigmoid(pre_gate)
    gate_act = pre_gate * gate_sig
    hidden = gate_act * pre_up
    hidden_grad = weight * along
    gate_grad = (hidden_grad * pre_up * gate_sig * (1.0 + pre_gate * (1.0 - gate_sig))).astype(
        jnp.bfloat16
    )
    up_grad = (hidden_grad * gate_act).astype(jnp.bfloat16)
    scaled = (weight * hidden).astype(jnp.bfloat16)
    grad_gate = jnp.einsum("rd,rf->df", rows, gate_grad, preferred_element_type=jnp.float32).astype(
        jnp.bfloat16
    )
    grad_up = jnp.einsum("rd,rf->df", rows, up_grad, preferred_element_type=jnp.float32).astype(
        jnp.bfloat16
    )
    grad_down = jnp.einsum("rf,rd->fd", scaled, back, preferred_element_type=jnp.float32).astype(
        jnp.bfloat16
    )
    row_part = jnp.einsum(
        "rf,df->rd", gate_grad, wgate, preferred_element_type=jnp.float32
    ) + jnp.einsum("rf,df->rd", up_grad, wup, preferred_element_type=jnp.float32)
    slot_part = jnp.sum(hidden * along, axis=1)
    row_share = sum_at_owner(
        row_part.reshape(experts, capacity, width).astype(jnp.bfloat16), "tp", 2
    )
    slot_sum = taken_together(slot_part.astype(jnp.bfloat16), "tp").astype(jnp.float32)
    back_grad = slot_sum.astype(jnp.bfloat16).reshape(experts, capacity)
    home_rows, home_grad = in_one_piece((row_share.astype(jnp.bfloat16), back_grad), "ep", 0, 0, 2)
    feature_part = jnp.einsum(
        "st,sd->td",
        by_token,
        home_rows.reshape(slot_total, home_rows.shape[2]),
        preferred_element_type=jnp.float32,
    ).astype(jnp.bfloat16)
    grad_tokens = gathered_copies(feature_part, "tp", 1)
    grad_weights = home_grad.reshape(-1)[target].reshape(local_tokens, top_count)
    return (grad_tokens, grad_weights, grad_gate[None], grad_up[None], grad_down[None])


def solution(mesh):
    return jax.shard_map(
        on_device,
        mesh=mesh,
        in_specs=(
            P("ep", None),
            P("ep", None),
            P("ep", None),
            P("ep", None),
            P("ep", None, "tp"),
            P("ep", None, "tp"),
            P("ep", "tp", None),
        ),
        out_specs=(
            P("ep", None),
            P("ep", None),
            P("ep", None, "tp"),
            P("ep", None, "tp"),
            P("ep", "tp", None),
        ),
        check_vma=False,
    )
```

profile of v0, /device:TPU:1, one launch (start us, length us, event | category | flops | bytes accessed | tf_op | source)
XLA Modules:
  0.0 262.2 jit_solution(12174575858582199878)
XLA Ops:
  7.2 0.9 copy.71
  8.4 0.9 reduce-window.6
  10.5 0.9 convert_reduce_fusion
  11.8 1.1 convolution_convert_fusion.4
  14.0 35.0 %all_to_all.26 = bf16[48,2,1285]{2,1,0:T(2,128)(2,1)S(1)} all-to-all(bf16[48,2,1285]{2,1,0:T(2,128)(2,1)S(1)} %reshape.144), channel_id=1, replica_groups=mesh['ep'=48,'tp'=16] {'ep'}, dimensions={0} | all-to-all | bytes 493440 | tf_op jit(solution)/shard_map/all_to_all | solution.py:11
  49.7 0.8 pad_maximum_fusion.1
  50.8 57.8 %all-gather.2.cloned.1.call-done = bf16[96,10,2048]{2,1,0:T(8,128)(2,1)} async-done(((bf16[96,10,128]{2,1,0:T(8,128)(2,1)}), bf16[96,10,2048]{2,1,0:T(8,128)(2,1)}) %all-gather.2.cloned.1.call-update) | async-done | bytes 3932176 | tf_op jit(solution)/shard_map/all_gather | solution.py:28
  108.6 6.6 %fusion.30 = (bf16[48,10,2048]{2,1,0:T(8,128)(2,1)}, bf16[48,10,2048]{2,1,0:T(8,128)(2,1)}) fusion(bf16[96,10,2048]{2,1,0:T(8,128)(2,1)} %all-gather.2.cloned.1.call-done), kind=kLoop, calls=%fused_computation.60 | loop fusion | bytes 7864320 | tf_op jit(solution)/shard_map/split | solution.py:28
  115.3 2.9 %reshape.127 = bf16[480,2048]{1,0:T(8,128)(2,1)S(1)} reshape(bf16[48,10,2048]{2,1,0:T(8,128)(2,1)} %get-tuple-element.37) | data formatting | bytes 3932160 | tf_op jit(solution)/shard_map/reshape | solution.py:105
  118.2 4.3 %reshape.126 = bf16[480,2048]{1,0:T(8,128)(2,1)} reshape(bf16[48,10,2048]{2,1,0:T(8,128)(2,1)} %get-tuple-element.38) | data formatting | bytes 3932160 | tf_op jit(solution)/shard_map/reshape | solution.py:106
  123.2 0.9 copy-done.1
  125.3 1.5 multiply_convert_fusion.2
  127.3 0.7 reduce.11
  128.7 5.5 %all-to-all-start.2 = ((bf16[16,2,240]{2,1,0:T(2,128)(2,1)}), bf16[16,2,240]{2,1,0:T(2,128)(2,1)S(1)}, u32[]{:S(2)}, u32[]{:S(2)}) async-start(bf16[16,2,240]{2,1,0:T(2,128)(2,1)} %reshape.146), calls=%async_computation.2 | async-start | bytes 32768 | tf_op jit(solution)/shard_map/all_to_all | solution.py:44
  134.2 1.8 fusion.4
  137.3 2.1 copy.91
  139.4 2.2 all-to-all-done.2
  141.5 5.1 %all-to-all-start.1 = ((bf16[16,48,10,128]{3,1,2,0:T(8,128)(2,1)}), bf16[16,48,10,128]{3,1,2,0:T(8,128)(2,1)}, u32[]{:S(2)}, u32[]{:S(2)}) async-start(bf16[16,48,10,128]{3,1,2,0:T(8,128)(2,1)} %bitcast.68), calls=%async_computation.1 | async-start | bytes 3932160 | tf_op jit(solution)/shard_map/all_to_all | solution.py:38
  147.0 46.1 %all-to-all-done.1 = bf16[16,48,10,128]{3,1,2,0:T(8,128)(2,1)} async-done(((bf16[16,48,10,128]{3,1,2,0:T(8,128)(2,1)}), bf16[16,48,10,128]{3,1,2,0:T(8,128)(2,1)}, u32[]{:S(2)}, u32[]{:S(2)}) %all-to-all-start.1) | async-done | bytes 1966112 | tf_op jit(solution)/shard_map/all_to_all | solution.py:38
  193.1 1.8 reduce_sum.68
  195.5 25.7 %all_to_all.27 = bf16[48,2,645]{2,1,0:T(2,128)(2,1)} all-to-all(bf16[48,2,645]{2,1,0:T(2,128)(2,1)S(1)} %reshape.148), channel_id=1, replica_groups=mesh['ep'=48,'tp'=16] {'ep'}, dimensions={0} | all-to-all | bytes 247680 | tf_op jit(solution)/shard_map/all_to_all | solution.py:11
  221.1 1.2 reshape.149
  223.2 1.1 convolution_convert_fusion.5
  224.3 1.0 broadcast_in_dim.21
  225.3 6.4 %all-to-all-start.4 = ((bf16[16,192,128]{2,1,0:T(8,128)(2,1)}), bf16[16,192,128]{2,1,0:T(8,128)(2,1)S(1)}, u32[]{:S(2)}, u32[]{:S(2)}) async-start(bf16[16,192,128]{2,1,0:T(8,128)(2,1)} %broadcast_in_dim.21), calls=%async_computation.4 | async-start | bytes 1572864 | tf_op jit(solution)/shard_map/all_to_all | solution.py:44
  231.7 1.0 mul.88
  232.8 2.6 %fusion = bf16[1,2048,128]{2,1,0:T(8,128)(2,1)} fusion(bf16[480,2048]{1,0:T(8,128)(2,1)S(1)} %reshape.127, bf16[480,128]{1,0:T(8,128)(2,1)} %get-tuple-element.39), kind=kOutput, calls=%fused_computation.5 | convolution fusion | flops 251920384 | bytes 2613248 | tf_op jit(solution)/shard_map/rd,rf->df/dot_general | solution.py:123
  235.4 1.6 fusion.1
  237.0 1.4 fusion.2
  238.7 2.8 %gather_fusion = bf16[384]{0:T(512)(128)(2,1)S(1)} fusion(bf16[480]{0:T(512)(128)(2,1)S(1)} %reshape_reshape.9, s32[1024]{0:T(1024)S(1)} %pad_clamp_fusion), kind=kCustom, calls=%fused_computation | custom fusion | bytes 3072 | tf_op jit(solution)/shard_map/gather | solution.py:149
  242.4 12.0 %all-to-all-done.4 = bf16[16,192,128]{2,1,0:T(8,128)(2,1)S(1)} async-done(((bf16[16,192,128]{2,1,0:T(8,128)(2,1)}), bf16[16,192,128]{2,1,0:T(8,128)(2,1)S(1)}, u32[]{:S(2)}, u32[]{:S(2)}) %all-to-all-start.4) | async-done | bytes 786464 | tf_op jit(solution)/shard_map/all_to_all | solution.py:44
  254.4 1.0 copy_bitcast_fusion.1
  (67 shorter events, 11.2 us)
Async XLA Ops:
  7.2 4.3 %copy-start = (bf16[192,2048]{1,0:T(8,128)(2,1)S(1)}, bf16[192,2048]{1,0:T(8,128)(2,1)}, u32[]{:S(2)}) copy-start(bf16[192,2048]{1,0:T(8,128)(2,1)} %param.8) | copy-start | bytes 2359300
  7.2 101.5 %all-gather.2.cloned.1.call-start = ((), (), s32[]{:S(2)}) async-start(), calls=%async_computation.5 | async-start | bytes 6684672 | tf_op jit(solution)/shard_map/all_gather | solution.py:28
  118.2 4.3 %copy-start.3 = (bf16[1,2048,128]{2,1,0:T(8,128)(2,1)S(1)}, bf16[1,2048,128]{2,1,0:T(8,128)(2,1)}, u32[]{:S(2)}) copy-start(bf16[1,2048,128]{2,1,0:T(8,128)(2,1)} %param.12) | copy-start | bytes 1572868
  122.5 1.5 copy-start.1
  122.5 1.6 copy-start.9
  124.1 2.6 copy-start.6
  124.1 1.1 copy-start.8
  128.7 12.8 %all-to-all-start.2 = ((bf16[16,2,240]{2,1,0:T(2,128)(2,1)}), bf16[16,2,240]{2,1,0:T(2,128)(2,1)S(1)}, u32[]{:S(2)}, u32[]{:S(2)}) async-start(bf16[16,2,240]{2,1,0:T(2,128)(2,1)} %reshape.146), calls=%async_computation.2 | async-start | bytes 32768 | tf_op jit(solution)/shard_map/all_to_all | solution.py:44
  134.2 1.8 copy-start.10
  141.5 51.6 %all-to-all-start.1 = ((bf16[16,48,10,128]{3,1,2,0:T(8,128)(2,1)}), bf16[16,48,10,128]{3,1,2,0:T(8,128)(2,1)}, u32[]{:S(2)}, u32[]{:S(2)}) async-start(bf16[16,48,10,128]{3,1,2,0:T(8,128)(2,1)} %bitcast.68), calls=%async_computation.1 | async-start | bytes 3932160 | tf_op jit(solution)/shard_map/all_to_all | solution.py:38
  222.4 2.9 %copy-start.4 = (bf16[48,10,129]{2,1,0:T(8,128)(2,1)}, bf16[48,10,129]{2,1,0:T(8,128)(2,1)S(1)}, u32[]{:S(2)}) copy-start(bf16[48,10,129]{2,1,0:T(8,128)(2,1)S(1)} %reshape.149) | copy-start | bytes 371524
  225.3 29.1 %all-to-all-start.4 = ((bf16[16,192,128]{2,1,0:T(8,128)(2,1)}), bf16[16,192,128]{2,1,0:T(8,128)(2,1)S(1)}, u32[]{:S(2)}, u32[]{:S(2)}) async-start(bf16[16,192,128]{2,1,0:T(8,128)(2,1)} %broadcast_in_dim.21), calls=%async_computation.4 | async-start | bytes 1572864 | tf_op jit(solution)/shard_map/all_to_all | solution.py:44
  232.7 2.7 %copy-start.11 = (bf16[480,128]{1,0:T(8,128)(2,1)S(1)}, bf16[480,128]{1,0:T(8,128)(2,1)}, u32[]{:S(2)}) copy-start(bf16[480,128]{1,0:T(8,128)(2,1)} %get-tuple-element.43) | copy-start | bytes 368644
  232.8 4.3 %copy-start.2 = (bf16[480,2048]{1,0:T(8,128)(2,1)S(1)}, bf16[480,2048]{1,0:T(8,128)(2,1)}, u32[]{:S(2)}) copy-start(bf16[480,2048]{1,0:T(8,128)(2,1)} %reshape.126) | copy-start | bytes 5898244
  232.8 4.3 %copy-start.7 = (f32[480,128]{1,0:T(8,128)S(1)}, f32[480,128]{1,0:T(8,128)}, u32[]{:S(2)}) copy-start(f32[480,128]{1,0:T(8,128)} %copy-done.6) | copy-start | bytes 737284
  232.8 4.3 %copy-start.12 = (f32[480,128]{1,0:T(8,128)S(1)}, f32[480,128]{1,0:T(8,128)}, u32[]{:S(2)}) copy-start(f32[480,128]{1,0:T(8,128)} %get-tuple-element.46) | copy-start | bytes 737284
  237.0 1.4 copy-start.5
Sparse Core Ops, SparseCore 0:
  50.6 57.9 all-gather.1
where the time goes:
time: 263 us; the launch traced here: 262 us
  waiting for transfers between devices  118 us (45%)
  blocking collectives  60.7 us (23%)
  local copies, waits for them, and re-layouts  32.2 us (12%)
  starting transfers between devices  17 us (6%)
  between operations  14.4 us (5%)
  matrix products  13.3 us (5%)
  other arithmetic  6.5 us (2%)
    all_to_all x2, blocking collectives, in_one_piece(): lax.all_to_all(both, axis, split_axis=split_dim, concat_axis=concat_dim,...  60.7 us
    all_gather x1, waiting for transfers between devices, in_one_piece_2(): lax.all_gather(both, axis, axis=dim, tiled=True)  57.8 us
    all_to_all x1, waiting for transfers between devices, sum_at_owner(): lax.all_to_all(tiles, axis, split_axis=0, concat_axis=0, tiled=True)  46.1 us
    all_to_all x2, waiting for transfers between devices, from_everyone(): return lax.all_to_all(copies, axis, split_axis=0, concat_axis=0, tiled=True)  14.2 us
    all_to_all x2, starting transfers between devices, from_everyone(): return lax.all_to_all(copies, axis, split_axis=0, concat_axis=0, tiled=True)  11.9 us
    unnamed x36, local copies, waits for them, and re-layouts  7.18 us
    split x1, local copies, waits for them, and re-layouts, in_one_piece_2(): jnp.split(lax.all_gather(both, axis, axis=dim, tiled=True), ends, axis=al...  6.64 us
  transfers between devices with their start and end apart: 4, of which 4 were waited for; matrix products, arithmetic and copies ran while one was open for 6% of the time, Pallas kernels for 0%

commit v1 on v0

v1 whole, which is shorter than its diff:
```python
import functools

import jax
import jax.numpy as jnp
from jax import lax
from jax.experimental import pallas as pl
from jax.experimental.pallas import tpu as pltpu
from jax.sharding import PartitionSpec as P

MESH = pl.DeviceIdType.MESH
BF = jnp.bfloat16
F32 = jnp.float32
CAP = 10
MSG = 24
RET = 16
NN = (((1,), (0,)), ((), ()))
NT = (((1,), (1,)), ((), ()))
TN = (((0,), (0,)), ((), ()))


def dot(a, b, dims=NN):
    return lax.dot_general(a, b, dims, preferred_element_type=F32)


def iota(shape, dim):
    return lax.broadcasted_iota(jnp.int32, shape, dim)


def remote(src, dst, send, recv, device):
    return pltpu.make_async_remote_copy(
        src_ref=src, dst_ref=dst, send_sem=send, recv_sem=recv,
        device_id=device, device_id_type=MESH)


def kernel(n_ep, n_tp, tok_h, cot_h, wg_h, wu_h, wd_h, rt, rtT, rwT,
           out, gw, ggate, gup, gdown,
           tok, cot, W, WD, WDT, WT, WTP, SO, SI, G, GG, GP, SC, SPR, TP, DS, DR, SM, RB, TM,
           in_sem, a_send, a_recv, w_sem, b_send, b_recv, m_send, m_recv, g_send, g_recv,
           d_send, d_recv, e_send, e_recv, f_send, f_recv, fm_send, fm_recv):
    ny = n_tp // 2
    nx = ny // 2
    nz = n_ep // nx
    km = n_ep // n_tp
    xbits = nx.bit_length() - 1
    width = tok.shape[1]
    half_w = width // 2
    ntok = tok.shape[0]
    hid = WD.shape[0]
    slots = n_tp * 32

    e = lax.axis_index("ep")
    t = lax.axis_index("tp")
    z, x = lax.div(e, nx), lax.rem(e, nx)
    y, c = lax.div(t, 2), lax.rem(t, 2)

    def at_y(step):
        return lax.rem(y + (step % ny), ny)

    def dev_y(step):
        return {"tp": at_y(step) * 2 + c}

    def dev_e(dz, dx):
        return {"ep": lax.rem(z + nz + dz, nz) * nx + lax.rem(x + nx + dx, nx)}

    mate = {"tp": y * 2 + 1 - c}

    loads = [
        pltpu.make_async_copy(tok_h, tok, in_sem.at[0]),
        pltpu.make_async_copy(cot_h, cot, in_sem.at[1]),
        pltpu.make_async_copy(wg_h, W.at[:, pl.ds(0, hid)], in_sem.at[2]),
        pltpu.make_async_copy(wu_h, W.at[:, pl.ds(hid, hid)], in_sem.at[3]),
        pltpu.make_async_copy(wd_h, WD, in_sem.at[4]),
    ]
    for copy in loads:
        copy.start()

    barrier = pltpu.get_barrier_semaphore()

    def greet(d, carry):
        pl.semaphore_signal(barrier, inc=1, device_id=dev_e(lax.div(d, nx), lax.rem(d, nx)), device_id_type=MESH)
        return carry

    lax.fori_loop(1, n_ep, greet, 0)
    for device in (dev_y(1), dev_y(-1), mate):
        pl.semaphore_signal(barrier, inc=1, device_id=device, device_id_type=MESH)
    others = n_ep - 1 + 3
    for step in range(2, ny - 1):
        pl.semaphore_signal(barrier, inc=1, device_id=dev_y(step), device_id_type=MESH)
        others += 1

    dz0 = 2 * c + lax.rem(y, 2)
    dx0 = lax.div(y, 2)
    rows = km * MSG
    ri = iota((rows, ntok), 0)
    kk = jnp.zeros((rows, ntok), jnp.int32)
    for k in range(1, km):
        kk = kk + (ri >= k * MSG).astype(jnp.int32)
    s_in = ri - kk * MSG
    ex = lax.rem(x + dx0, nx)
    want = jnp.zeros((rows, ntok), jnp.int32)
    for k in range(km):
        expert_k = lax.rem(z + dz0 + 4 * k, nz) * nx + ex
        want = jnp.where(kk == k, expert_k, want)
    hit0 = rtT[0:1, :] == want
    hit1 = rtT[1:2, :] == want
    hit = jnp.where(hit0 | hit1, 1.0, 0.0)
    before = jnp.where(iota((ntok, ntok), 0) < iota((ntok, ntok), 1), 1.0, 0.0).astype(BF)
    rank = dot(hit.astype(BF), before).astype(jnp.int32)
    q_tok = jnp.where(rank == s_in, hit, 0.0)
    q_cot = jnp.where(rank + CAP == s_in, hit, 0.0)
    q_cot = jnp.where(s_in >= CAP, q_cot, 0.0)
    q_cot = jnp.where(s_in < 2 * CAP, q_cot, 0.0)
    q_tok = jnp.where(s_in < CAP, q_tok, 0.0)
    w_hit = jnp.where(hit0, rwT[0:1, :], rwT[1:2, :]).astype(BF).astype(F32)
    w_col = jnp.sum(q_tok * w_hit, axis=1, keepdims=True)
    li = iota((rows, 128), 1)
    ri1 = iota((rows, 128), 0)
    kk1 = jnp.zeros((rows, 128), jnp.int32)
    for k in range(1, km):
        kk1 = kk1 + (ri1 >= k * MSG).astype(jnp.int32)
    s1 = ri1 - kk1 * MSG
    w_diag = jnp.where((li == kk1 * CAP + s1) & (s1 < CAP), w_col, 0.0).astype(BF)
    rr, rc = iota((rows, rows), 0), iota((rows, rows), 1)
    collect = jnp.zeros((rows, rows), F32)
    for k in range(km):
        collect = jnp.where((rr == k * MSG + 2 * CAP) & (rc >= k * MSG) & (rc < k * MSG + MSG), 1.0, collect)
    w_rows = dot(collect.astype(BF), w_diag)
    q_tok = q_tok.astype(BF)
    q_cot = q_cot.astype(BF)
    loads[0].wait()
    loads[1].wait()
    tile = min(512, width)
    for j in range(width // tile):
        cols = slice(j * tile, (j + 1) * tile)
        part = dot(q_tok, tok[:, cols]) + dot(q_cot, cot[:, cols])
        SO[:, cols] = part.astype(BF)
        if j == 0:
            SO[:, 0:128] = (part[:, 0:128] + w_rows).astype(BF)

    pl.semaphore_wait(barrier, others)

    def a_copy(k):
        return remote(SO.at[pl.ds(k * MSG, MSG)], SI.at[pl.ds(k * MSG, MSG)], a_send.at[k], a_recv.at[k],
                      dev_e(dz0 + 4 * k, dx0))

    order = [k for k in range(km) if k == 1] + [k for k in range(km) if k != 1]
    for k in order:
        if k == 0:
            @pl.when(t != 0)
            def _():
                a_copy(0).start()

            @pl.when(t == 0)
            def _():
                SI[0:MSG, :] = SO[0:MSG, :]
        else:
            a_copy(k).start()

    for copy in loads[2:]:
        copy.wait()
    for j in range(n_tp):
        WT[j % 2, j // 2] = W[j * 128:(j + 1) * 128, :].T
        WDT[j * 128:(j + 1) * 128, :] = WD[:, j * 128:(j + 1) * 128].T
    w_copy = remote(WT.at[1 - c], WTP, w_sem.at[0], w_sem.at[1], mate)
    w_copy.start()

    lane = iota((ntok, 128), 1)
    r0, r1 = rt[:, 0:1], rt[:, 1:2]

    def entry_places():
        h0, h1 = r0 == lane, r1 == lane
        named = jnp.where(h0 | h1, 1.0, 0.0).astype(BF)
        lower = jnp.where(iota((ntok, ntok), 1) < iota((ntok, ntok), 0), 1.0, 0.0).astype(BF)
        count = dot(lower, named)
        n0 = jnp.sum(jnp.where(h0, count, 0.0), axis=1, keepdims=True).astype(jnp.int32)
        n1 = jnp.sum(jnp.where(h1, count, 0.0), axis=1, keepdims=True).astype(jnp.int32)

        def place(r, n):
            dz = (r >> xbits) - z
            dz = jnp.where(dz < 0, dz + nz, dz)
            dx = ((r & (nx - 1)) + nx - x) & (nx - 1)
            group = 4 * dx + 2 * (dz & 1) + ((dz >> 1) & 1)
            k = dz >> 2
            return (group * km + k) * RET, (group & 3) * 32 + k * CAP + n

        m0, l0 = place(r0, n0)
        m1, l1 = place(r1, n1)
        return m0, n0, l0, m1, n1, l1

    m0, n0, _, m1, n1, _ = entry_places()
    for j in range(n_ep * RET // 128):
        col = lane + 128 * j
        TM[:, j * 128:(j + 1) * 128] = jnp.where((col == m0 + n0) | (col == m1 + n1), 1.0, 0.0).astype(BF)

    pr, pc = iota((64, rows), 0), iota((64, rows), 1)
    pack = jnp.zeros((64, rows), F32)
    for k in range(km):
        lo = k * CAP
        pack = jnp.where((pr >= lo) & (pr < lo + CAP) & (pc == pr - lo + k * MSG), 1.0, pack)
        pack = jnp.where((pr == 30) & (pc == k * MSG + 2 * CAP), 1.0, pack)
        pack = jnp.where((pr >= 32 + lo) & (pr < 32 + lo + CAP) & (pc == pr - 32 - lo + k * MSG + CAP), 1.0, pack)
    pack = pack.astype(BF)
    for k in order:
        if k == 0:
            @pl.when(t != 0)
            def _():
                a_copy(0).wait()
        else:
            a_copy(k).wait()
    mine = pl.ds(pl.multiple_of(t * 32, 32), 32)
    htile = min(512, half_w)
    for j in range(width // htile):
        part = dot(pack, SI[:, j * htile:(j + 1) * htile]).astype(BF)
        h, off = (j * htile) // half_w, (j * htile) % half_w
        G[0, h, mine, off:off + htile] = part[0:32]
        G[1, h, mine, off:off + htile] = part[32:64]

    long_hops, short_hops = ny // 2, ny // 2 - 1
    flows = [(1, 0, long_hops), (-1, 1, long_hops), (1, 1, short_hops), (-1, 0, short_hops)]
    pieces = {}
    for sgn, h, hops in flows:
        for s in range(1, hops + 1):
            pieces[(sgn, h, s)] = len(pieces)

    def piece(h, yo):
        return G.at[:, h, pl.ds(pl.multiple_of((yo * 2 + c) * 32, 32), 32), :]

    def ring(sgn, h, s):
        i = pieces[(sgn, h, s)]
        yo = at_y(-sgn * (s - 1))
        return remote(piece(h, yo), piece(h, yo), b_send.at[i], b_recv.at[i], dev_y(sgn))

    def share(i, h, yo):
        return remote(piece(h, yo), piece(h, yo), m_send.at[i], m_recv.at[i], mate)

    for sgn, h, hops in flows:
        ring(sgn, h, 1).start()
    for h in range(2):
        share(len(pieces) + h, h, y).start()

    def expert(yo, sem):
        here = pl.ds(pl.multiple_of(yo * 64, 64), 64)
        ra, rb = G[0, 0, here, :], G[0, 1, here, :]
        pre = dot(ra, W[0:half_w, :]) + dot(rb, W[half_w:, :])
        along = dot(G[1, 0, here, :], WDT[0:half_w, :]) + dot(G[1, 1, here, :], WDT[half_w:, :])
        pre_gate, pre_up = pre[:, 0:hid], pre[:, hid:]
        wf = ra[:, 0:128].astype(F32)
        row, col = iota((64, 128), 0), iota((64, 128), 1)
        wf = jnp.where(row < 32, wf[30:31, :], wf[62:63, :])
        weight = jnp.sum(jnp.where((row & 31) == col, wf, 0.0), axis=1, keepdims=True)
        sig = jax.nn.sigmoid(pre_gate)
        act = pre_gate * sig
        hidden = act * pre_up
        hidden_grad = weight * along
        gate_grad = hidden_grad * pre_up * sig * (1.0 + pre_gate * (1.0 - sig))
        GG[here, 0:hid] = gate_grad.astype(BF)
        GG[here, hid:2 * hid] = (hidden_grad * act).astype(BF)
        part = jnp.sum(hidden * along, axis=1, keepdims=True)
        GG[here, 2 * hid:3 * hid] = jnp.broadcast_to(part, (64, hid)).astype(BF)
        SC[here, :] = (weight * hidden).astype(BF)
        grads(yo, sem).start()

    def grads(yo, sem):
        here = pl.ds(pl.multiple_of(yo * 64, 64), 64)
        return remote(GG.at[here], GP.at[here], g_send.at[sem], g_recv.at[sem], mate)

    for h in range(2):
        share(len(pieces) + h, h, y).wait_recv()
    expert(y, 0)
    for s in range(1, long_hops + 1):
        for sgn, h, hops in flows:
            if s <= hops:
                i = pieces[(sgn, h, s)]
                yo = at_y(-sgn * s)
                remote(piece(h, yo), piece(h, yo), b_send.at[i], b_recv.at[i], dev_y(sgn)).wait_recv()
                if s < hops:
                    ring(sgn, h, s + 1).start()
                share(i, h, yo).start()
        for sgn, h, hops in flows:
            if s <= hops:
                share(pieces[(sgn, h, s)], h, at_y(-sgn * s)).wait_recv()
        expert(at_y(-s), s)
        if s < long_hops:
            expert(at_y(s), ny - s)

    w_copy.wait()
    grads(y, 0).wait()
    for s in range(1, long_hops + 1):
        grads(at_y(-s), s).wait()
        if s < long_hops:
            grads(at_y(s), ny - s).wait()

    nq = 4
    quarter = slots // nq

    def row_part(j):
        yt = at_y(j)
        for p in range(2):
            cut = slice(p * slots // 2, (p + 1) * slots // 2)
            TP[j % ny, cut, :] = dot(GG[cut, 0:2 * hid], WT[c, yt]) + dot(GP[cut, 0:2 * hid], WTP[yt])

    row_part(long_hops)
    for q in range(nq):
        cut = slice(q * quarter, (q + 1) * quarter)
        both = GG[cut, 2 * hid:3 * hid].astype(F32) + GP[cut, 2 * hid:3 * hid].astype(F32)
        diag = jnp.where(iota((quarter, 128), 0) == iota((quarter, 128), 1), both[:, 0:128], 0.0)
        SPR[q] = jnp.broadcast_to(jnp.sum(diag, axis=0, keepdims=True), (8, 128))

    def hops_of(sgn, q):
        return long_hops if (sgn > 0) == (q < nq // 2) else short_hops

    parts = {}
    for sgn in (1, -1):
        for q in range(nq):
            for s in range(1, hops_of(sgn, q) + 1):
                parts[(sgn, q, s)] = len(parts)

    def d_copy(sgn, q, s):
        i = parts[(sgn, q, s)]
        return remote(DS.at[i], DR.at[i], d_send.at[i], d_recv.at[i], dev_y(sgn))

    def hop(sgn, q, s):
        i = parts[(sgn, q, s)]
        target = sgn * (hops_of(sgn, q) + 1 - s)
        val = TP[target % ny, q * quarter:(q + 1) * quarter, :]
        slot = SPR[q]
        if s > 1:
            d_copy(sgn, q, s - 1).wait_recv()
            j = parts[(sgn, q, s - 1)]
            val = val + DR[j, 0:quarter, :].astype(F32)
            slot = slot + DR[j, quarter:, :].astype(F32)
        DS[i, 0:quarter, :] = val.astype(BF)
        DS[i, quarter:, :] = slot.astype(BF)
        d_copy(sgn, q, s).start()

    low, high = range(nq // 2), range(nq // 2, nq)
    for q in range(nq // 2):
        hop(1, q, 1)
        hop(-1, q + nq // 2, 1)
    row_part(short_hops)
    for q in high:
        hop(1, q, 1)
    row_part(-short_hops)
    for q in low:
        hop(-1, q, 1)
    for s in range(2, long_hops + 1):
        if short_hops + 1 - s >= 0:
            row_part(short_hops + 1 - s)
            if short_hops + 1 - s > 0:
                row_part(-(short_hops + 1 - s))
        for q in range(nq // 2):
            hop(1, q, s)
            hop(-1, q + nq // 2, s)
        if s <= short_hops:
            for q in range(nq // 2):
                hop(1, q + nq // 2, s)
                hop(-1, q, s)

    e_rows = slots // nq // 32 * km * RET
    ur, uc = iota((e_rows, quarter + 8), 0), iota((e_rows, quarter + 8), 1)
    unpack = jnp.zeros((e_rows, quarter + 8), F32)
    for m in range(e_rows // RET):
        base = (m // km) * 32 + (m % km) * CAP
        lo = m * RET
        unpack = jnp.where((ur >= lo) & (ur < lo + CAP) & (uc == ur - lo + base), 1.0, unpack)
        unpack = jnp.where((ur == lo + CAP) & (uc == quarter), 1.0, unpack)
    unpack = unpack.astype(BF)
    per_q = e_rows // RET
    for q in range(nq):
        val = TP[0, q * quarter:(q + 1) * quarter, :]
        slot = SPR[q]
        for sgn in (1, -1):
            last = hops_of(sgn, q)
            d_copy(sgn, q, last).wait_recv()
            j = parts[(sgn, q, last)]
            val = val + DR[j, 0:quarter, :].astype(F32)
            slot = slot + DR[j, quarter:, :].astype(F32)
        total = jnp.concatenate([val, slot], axis=0).astype(BF)
        messages = dot(unpack, total).astype(BF)
        SM[q * e_rows:(q + 1) * e_rows, :] = messages
        if q == 0:
            RB[0:RET, :] = messages[0:RET]
        for m in range(per_q):
            i = q * per_q + m
            if i == 0:
                continue
            group, k = i // km, i % km
            dx, rem = group // 4, group % 4
            dz = 4 * k + 2 * (rem % 2) + rem // 2
            place = pl.ds(i * RET, RET)
            remote(SM.at[place], RB.at[place], e_send, e_recv, dev_e(-dz, -dx)).start()

    for h in range(2):
        for j in range(half_w // 256):
            cols = slice(j * 256, (j + 1) * 256)
            there = slice(h * half_w + j * 256, h * half_w + (j + 1) * 256)
            both = dot(G[0, h, :, cols], GG[:, 0:2 * hid], TN)
            ggate[there, :] = both[:, 0:hid].astype(BF)
            gup[there, :] = both[:, hid:].astype(BF)
            gdown[:, there] = dot(SC[...], G[1, h, :, cols], TN).astype(BF)

    rest = pl.ds(RET, (n_ep - 1) * RET)
    home = remote(SM.at[rest], RB.at[rest], e_send, e_recv, mate)
    home.wait_recv()

    def features(step, same=True):
        to = at_y(step) * 2 + c
        return out.at[:, pl.ds(pl.multiple_of(to * 128, 128), 128)]

    out[:, pl.ds(pl.multiple_of(t * 128, 128), 128)] = dot(TM[...], RB[...]).astype(BF)

    def f_copy(i, step):
        return remote(features(0), features(0), f_send.at[i], f_recv.at[i], dev_y(step))

    far_first = sorted(range(1, ny), key=lambda s: -min(s, ny - s))
    for i, step in enumerate(far_first):
        f_copy(i, step).start()

    def pass_on(i, step):
        return remote(features(step), features(step), fm_send.at[i], fm_recv.at[i], mate)

    pass_on(ny - 1, 0).start()

    m0, n0, l0, m1, n1, l1 = entry_places()
    got0 = jnp.zeros((ntok, 128), F32)
    got1 = jnp.zeros((ntok, 128), F32)
    for j in range(n_ep * RET // 128):
        col = lane + 128 * j
        there = RB[j * 128:(j + 1) * 128, :]
        got0 = got0 + dot(jnp.where(col == m0 + CAP, 1.0, 0.0).astype(BF), there)
        got1 = got1 + dot(jnp.where(col == m1 + CAP, 1.0, 0.0).astype(BF), there)
    w0 = jnp.sum(jnp.where(lane == l0, got0, 0.0), axis=1, keepdims=True)
    w1 = jnp.sum(jnp.where(lane == l1, got1, 0.0), axis=1, keepdims=True)
    gw[...] = jnp.where(iota((ntok, 2), 1) == 0, w0, w1).astype(BF)

    near_first = sorted(range(1, ny), key=lambda s: min(s, ny - s))
    for step in near_first:
        i = far_first.index(step)
        back = far_first.index((-step) % ny)
        remote(features(step), features(step), f_send.at[back], f_recv.at[back], dev_y(-step)).wait_recv()
        pass_on(i, step).start()
    pass_on(ny - 1, 0).wait_recv()
    for step in near_first:
        pass_on(far_first.index(step), step).wait_recv()

    for (sgn, h, s), i in pieces.items():
        ring(sgn, h, s).wait_send()
        share(i, h, at_y(-sgn * s)).wait_send()
    for h in range(2):
        share(len(pieces) + h, h, y).wait_send()
    for key in parts:
        d_copy(*key).wait_send()
    home.wait_send()
    for i, step in enumerate(far_first):
        f_copy(i, step).wait_send()
        pass_on(i, step).wait_send()
    pass_on(ny - 1, 0).wait_send()


def on_device(n_ep, n_tp, tokens, cotangent, routing, route_weights, w_gate, w_up, w_down):
    ntok, width = tokens.shape
    hid = w_gate.shape[2]
    ny = n_tp // 2
    km = n_ep // n_tp
    slots = n_tp * 32
    pieces = 2 * (ny - 1)
    parts = 4 * (ny - 1)
    vmem = pl.BlockSpec(memory_space=pltpu.VMEM)
    hbm = pl.BlockSpec(memory_space=pl.ANY)
    dma = pltpu.SemaphoreType.DMA
    grad_tokens, grad_weights, grad_gate, grad_up, grad_down = pl.pallas_call(
        functools.partial(kernel, n_ep, n_tp),
        out_shape=(
            jax.ShapeDtypeStruct((ntok, width), BF),
            jax.ShapeDtypeStruct((ntok, 2), BF),
            jax.ShapeDtypeStruct((width, hid), BF),
            jax.ShapeDtypeStruct((width, hid), BF),
            jax.ShapeDtypeStruct((hid, width), BF),
        ),
        in_specs=[hbm] * 5 + [vmem] * 3,
        out_specs=[vmem] * 5,
        scratch_shapes=[
            pltpu.VMEM((ntok, width), BF),
            pltpu.VMEM((ntok, width), BF),
            pltpu.VMEM((width, 2 * hid), BF),
            pltpu.VMEM((hid, width), BF),
            pltpu.VMEM((width, hid), BF),
            pltpu.VMEM((2, ny, 2 * hid, 128), BF),
            pltpu.VMEM((ny, 2 * hid, 128), BF),
            pltpu.VMEM((km * MSG, width), BF),
            pltpu.VMEM((km * MSG, width), BF),
            pltpu.VMEM((2, 2, slots, width // 2), BF),
            pltpu.VMEM((slots, 3 * hid), BF),
            pltpu.VMEM((slots, 3 * hid), BF),
            pltpu.VMEM((slots, hid), BF),
            pltpu.VMEM((4, 8, 128), F32),
            pltpu.VMEM((ny, slots, 128), F32),
            pltpu.VMEM((parts, slots // 4 + 8, 128), BF),
            pltpu.VMEM((parts, slots // 4 + 8, 128), BF),
            pltpu.VMEM((n_ep * RET, 128), BF),
            pltpu.VMEM((n_ep * RET, 128), BF),
            pltpu.VMEM((ntok, n_ep * RET), BF),
            dma((5,)),
            dma((km,)), dma((km,)),
            dma((2,)),
            dma((pieces,)), dma((pieces,)),
            dma((pieces + 2,)), dma((pieces + 2,)),
            dma((ny,)), dma((ny,)),
            dma((parts,)), dma((parts,)),
            dma, dma,
            dma((ny - 1,)), dma((ny - 1,)),
            dma((ny,)), dma((ny,)),
        ],
        compiler_params=pltpu.CompilerParams(
            collective_id=0, has_side_effects=True, vmem_limit_bytes=56 * 1024 * 1024),
    )(tokens, cotangent, w_gate[0], w_up[0], w_down[0], routing, routing.T, route_weights.T)
    return (grad_tokens, grad_weights, grad_gate[None], grad_up[None], grad_down[None])


def solution(mesh):
    n_ep, n_tp = mesh.shape["ep"], mesh.shape["tp"]
    return jax.shard_map(
        functools.partial(on_device, n_ep, n_tp),
        mesh=mesh,
        in_specs=(
            P("ep", None),
            P("ep", None),
            P("ep", None),
            P("ep", None),
            P("ep", None, "tp"),
            P("ep", None, "tp"),
            P("ep", "tp", None),
        ),
        out_specs=(
            P("ep", None),
            P("ep", None),
            P("ep", None, "tp"),
            P("ep", None, "tp"),
            P("ep", "tp", None),
        ),
        check_vma=False,
    )
```

time: 263 us -> 106 us (0.40)
  waiting for transfers between devices: 118 us -> 0 us
  Pallas kernels: 0 us -> 97.1 us
  blocking collectives: 60.7 us -> 0 us
  local copies, waits for them, and re-layouts: 32.2 us -> 8.3 us
  starting transfers between devices: 17 us -> 0 us
  between operations: 14.4 us -> 0.65 us
  matrix products: 13.3 us -> 0 us
  other arithmetic: 6.5 us -> 0 us
    pallas_call x0 -> x1, Pallas kernels: none -> 97.1 us  [on_device(): pl.pallas_call(functools.partial(kernel, n_ep, n_tp), out_shape=(jax.Shap...]
    all_to_all x2 -> x0, blocking collectives: 60.7 us -> none  [in_one_piece(): lax.all_to_all(both, axis, split_axis=split_dim, concat_axis=concat_dim,...]
    all_to_all x3 -> x0, waiting for transfers between devices: 60.3 us -> none  [the longest x1 46.1 us: sum_at_owner(): lax.all_to_all(tiles, axis, split_axis=0, concat_axis=0, tiled=True)]
    all_gather x1 -> x0, waiting for transfers between devices: 57.8 us -> none  [in_one_piece_2(): lax.all_gather(both, axis, axis=dim, tiled=True)]
    all_to_all x3 -> x0, starting transfers between devices: 16.9 us -> none  [the longest x2 11.9 us: from_everyone(): return lax.all_to_all(copies, axis, split_axis=0, concat_axis=0, tiled=True)]
    dot_general x11 -> x0, matrix products: 13.3 us -> none  [the longest x1 2.64 us: on_device(): jnp.einsum('rd,rf->df', rows, gate_grad, preferred_element_type=jnp.float32)]
    reshape x7 -> x0, local copies, waits for them, and re-layouts: 9.17 us -> none  [the longest x1 4.28 us: on_device(): back = back_in.reshape(slot_total, width)]
    split x1 -> x0, local copies, waits for them, and re-layouts: 6.64 us -> none  [in_one_piece_2(): jnp.split(lax.all_gather(both, axis, axis=dim, tiled=True), ends, axis=al...]
  transfers between devices with their start and end apart: 4 -> 0, of which waited for: 4 -> 0; matrix products, arithmetic and copies ran while one was open for 6% -> 0% of each run, Pallas kernels for 0% -> 0%
where the time goes in v1:
time: 106 us
  Pallas kernels  97.1 us (92%)
  local copies, waits for them, and re-layouts  8.3 us (8%)
    pallas_call x1, Pallas kernels, on_device(): pl.pallas_call(functools.partial(kernel, n_ep, n_tp), out_shape=(jax.Shap...  97.1 us
    unnamed x14, local copies, waits for them, and re-layouts  8.3 us

profile of v1, /device:TPU:1, one launch (start us, length us, event | category | flops | bytes accessed | tf_op | source)
XLA Modules:
  0.0 106.1 jit_solution(13070075859028329718)
XLA Ops:
  0.6 0.0 copy-start.3
  0.6 0.7 copy-done.3
  1.3 0.8 copy.12.rt
  2.1 97.1 %shard_map.110 = (bf16[192,2048]{1,0:T(8,128)(2,1)}, bf16[192,2]{1,0:T(8,128)(2,1)}, bf16[2048,128]{1,0:T(8,128)(2,1)}, bf16[2048,128]{1,0:T(8,128)(2,1)}, bf16[128,2048]{1,0:T(8,128)(2,1)}) custom-call(bf16[192,2048]{1,0:T(8,128)(2,1)} %tok_h.1, bf16[192,2048]{1,0:T(8,128)(2,1)} %cot_h.1, bf16[2048,128]{1,0:T(8,128)(2,1)} %bitcast.8, ...), custom_call_target="tpu_custom_call" | custom-call | tf_op jit(solution)/shard_map/pallas_call | solution.py:471
  99.2 1.5 %copy.13 = bf16[192,2]{0,1:T(2,128)(2,1)} copy(bf16[192,2]{1,0:T(8,128)(2,1)} %get-tuple-element.16) | data formatting | bytes 1536
  100.7 0.0 copy-start.2
  100.7 2.1 %copy.18 = bf16[192,2048]{1,0:T(8,128)(2,1)} copy(bf16[192,2048]{1,0:T(8,128)(2,1)} %get-tuple-element.25) | data formatting | bytes 1572864
  102.8 0.0 copy-done.2
  102.8 0.0 copy-start.1
  102.8 0.8 copy.19
  103.6 0.4 copy-done.1
  104.0 0.0 copy-start
  104.0 0.8 copy.20
  104.8 0.4 copy-done
  105.3 0.8 copy.21
Async XLA Ops:
  0.6 0.7 copy-start.3
  100.7 2.2 %copy-start.2 = (bf16[2048,128]{1,0:T(8,128)(2,1)S(1)}, bf16[2048,128]{1,0:T(8,128)(2,1)}, u32[]{:S(2)}) copy-start(bf16[2048,128]{1,0:T(8,128)(2,1)} %get-tuple-element.12) | copy-start | bytes 1572868
  102.8 1.2 %copy-start.1 = (bf16[2048,128]{1,0:T(8,128)(2,1)S(1)}, bf16[2048,128]{1,0:T(8,128)(2,1)}, u32[]{:S(2)}) copy-start(bf16[2048,128]{1,0:T(8,128)(2,1)} %get-tuple-element.13) | copy-start | bytes 1572868
  104.0 1.2 %copy-start = (bf16[128,2048]{1,0:T(8,128)(2,1)S(1)}, bf16[128,2048]{1,0:T(8,128)(2,1)}, u32[]{:S(2)}) copy-start(bf16[128,2048]{1,0:T(8,128)(2,1)} %get-tuple-element.14) | copy-start | bytes 1572868
